TPU v7x, 32 devices: a whole 2x2x4 slice. The times are simulated.
32 devices in a mesh: ep: 8 (over z, x), tp: 4 (over y, core).
Axes of the slice: x: 2, y: 2, z: 4, core: 2. Of those that a mesh axis runs over, the one named last changes fastest.
Arguments:
- hidden_in: bfloat16 [256, 2048], P('ep', 'tp'), may hold values from -6 to 6
- state_in: float32 [256, 8, 128, 128], P('ep', 'tp'), may hold values from -0.6 to 0.6
- attn_gain: float32 [2048], replicated, may hold values from 0.1 to 1.9
- w_query: bfloat16 [2048, 1024], P(None, 'tp'), may hold values from -0.125 to 0.125
- w_key: bfloat16 [2048, 1024], P(None, 'tp'), may hold values from -0.125 to 0.125
- w_value: bfloat16 [2048, 1024], P(None, 'tp'), may hold values from -0.125 to 0.125
- w_gate: bfloat16 [2048, 1024], P(None, 'tp'), may hold values from -0.125 to 0.125
- w_beta: bfloat16 [2048, 8], replicated, may hold values from -0.125 to 0.125
- w_decay: bfloat16 [2048, 8], replicated, may hold values from -0.125 to 0.125
- decay_scale: float32 [8], replicated, may hold values from 0.05 to 3
- head_gain: float32 [128], replicated, may hold values from 0.1 to 1.9
- w_output: bfloat16 [1024, 2048], P(None, 'tp'), may hold values from -0.1875 to 0.1875
- ffn_gain: float32 [2048], replicated, may hold values from 0.1 to 1.9
- expert_ids: int32 [256, 2], P('ep'), may hold values from 0 to 7, all different within a row; in each aligned block of 32 rows (0 to 31, 32 to 63, ...) at most 16 rows name the same one
- route_weight: float32 [256, 2], P('ep'), may hold values from 0.2 to 1
- expert_gate: bfloat16 [8, 2048, 3072], P('ep', None, 'tp'), may hold values from -0.125 to 0.125
- expert_up: bfloat16 [8, 2048, 3072], P('ep', None, 'tp'), may hold values from -0.125 to 0.125
- expert_down: bfloat16 [8, 3072, 2048], P('ep', 'tp'), may hold values from -0.109375 to 0.109375
- dense_gate: bfloat16 [2048, 4096], P(None, 'ep'), may hold values from -0.125 to 0.125
- dense_up: bfloat16 [2048, 4096], P(None, 'ep'), may hold values from -0.125 to 0.125
- dense_down: bfloat16 [4096, 2048], P('ep'), may hold values from -0.09375 to 0.09375
- dense_mix: float32 [2048], P('tp'), may hold values from -6 to 6
Outputs:
- result: bfloat16 [256, 2048], P('ep', 'tp')
- new_state: float32 [256, 8, 128, 128], P('ep', 'tp')
Inputs may be any that keep to these rules, and one draw needn't show every extreme that they name: `expert_ids`: each row names 2 different experts. Within the rows of one index of ep (aligned blocks of 32 sequences) no expert is named more than 16 times, a bound that some block reaches.
All inputs are finite; a program needn't handle non-finite values.
Results may differ from a plain program's by a relative error of at most 0.015.
Values may be sent and summed in bfloat16 or wider, within the bound.
A program may use at most 64 MiB of HBM per device.

v0:
```python
import functools

import jax
import jax.numpy as jnp
from jax import lax
from jax.experimental import pallas as pl
from jax.experimental.pallas import tpu as pltpu
from jax.sharding import PartitionSpec as P

EPS = 1e-06


def root_norm(values, scale_vec):
    wide = values.astype(jnp.float32)
    return wide * lax.rsqrt(jnp.mean(wide * wide, axis=-1, keepdims=True) + EPS) * scale_vec


def unit_norm(values):
    return values * lax.rsqrt(jnp.sum(values * values, axis=-1, keepdims=True) + EPS)


def slot_table(expert_ids, count):
    flat = expert_ids.reshape(-1)
    onehot = (flat[:, None] == jnp.arange(count, dtype=jnp.int32)[None, :]).astype(jnp.int32)
    before = jnp.cumsum(onehot, axis=0) - onehot
    return jnp.sum(before * onehot, axis=1).reshape(expert_ids.shape)


def delta_update(old_state, key_rows, value_rows, beta_rate, decay_rate):
    recalled = jnp.einsum("shk,shkv->shv", key_rows, old_state, precision=lax.Precision.HIGHEST)
    erased = (
        old_state - beta_rate[..., None, None] * key_rows[..., :, None] * recalled[..., None, :]
    )
    written = beta_rate[..., None, None] * key_rows[..., :, None] * value_rows[..., None, :]
    return decay_rate[..., None, None] * erased + written


def head_output(new_state, queries, gate_rows, head_gain):
    read = jnp.einsum("shk,shkv->shv", queries, new_state, precision=lax.Precision.HIGHEST)
    return (root_norm(read, head_gain) * jax.nn.silu(gate_rows)).astype(jnp.bfloat16)


def per_device(
    hidden_in,
    state_in,
    attn_gain,
    w_query,
    w_key,
    w_value,
    w_gate,
    w_beta,
    w_decay,
    decay_scale,
    head_gain,
    w_output,
    ffn_gain,
    expert_ids,
    route_weight,
    expert_gate,
    expert_up,
    expert_down,
    dense_gate,
    dense_up,
    dense_down,
    dense_mix,
):
    seq_dev = hidden_in.shape[0]
    tp_size = lax.axis_size("tp")
    ep_size = lax.axis_size("ep")
    tp_index = lax.axis_index("tp")
    local_heads = state_in.shape[1]
    key_dim = state_in.shape[2]
    value_dim = state_in.shape[3]
    local_width = hidden_in.shape[1]
    model_width = local_width * tp_size
    full_rows = lax.all_gather(hidden_in, "tp", axis=1, tiled=True)
    normed = root_norm(full_rows, attn_gain).astype(jnp.bfloat16)
    queries = unit_norm(
        jnp.dot(normed, w_query, preferred_element_type=jnp.float32).reshape(
            seq_dev, local_heads, key_dim
        )
    ) * key_dim ** (-0.5)
    key_rows = unit_norm(
        jnp.dot(normed, w_key, preferred_element_type=jnp.float32).reshape(
            seq_dev, local_heads, key_dim
        )
    )
    value_rows = jnp.dot(normed, w_value, preferred_element_type=jnp.float32).reshape(
        seq_dev, local_heads, value_dim
    )
    gate_rows = jnp.dot(normed, w_gate, preferred_element_type=jnp.float32).reshape(
        seq_dev, local_heads, value_dim
    )
    head_start = tp_index * local_heads
    beta_all = jnp.dot(normed, w_beta, preferred_element_type=jnp.float32)
    decay_all = jnp.dot(normed, w_decay, preferred_element_type=jnp.float32)
    beta_rate = jax.nn.sigmoid(lax.dynamic_slice_in_dim(beta_all, head_start, local_heads, 1))
    decay_logit = lax.dynamic_slice_in_dim(decay_all, head_start, local_heads, 1)
    decay_local = lax.dynamic_slice_in_dim(decay_scale, head_start, local_heads, 0)
    decay_rate = jnp.exp(-decay_local[None, :] * jax.nn.softplus(decay_logit))
    new_state = delta_update(state_in, key_rows, value_rows, beta_rate, decay_rate)
    heads_out = head_output(new_state, queries, gate_rows, head_gain).reshape(
        seq_dev, local_heads * value_dim
    )
    all_heads = lax.all_gather(heads_out, "tp", axis=1, tiled=True)
    mixed = (
        hidden_in.astype(jnp.float32)
        + jnp.dot(all_heads, w_output, preferred_element_type=jnp.float32)
    ).astype(jnp.bfloat16)
    block_rows = seq_dev // tp_size
    top_count = expert_ids.shape[1]
    experts_all = expert_gate.shape[0] * ep_size
    capacity = max(2, 2 * seq_dev * top_count // experts_all)
    slots = slot_table(expert_ids, experts_all)
    place = expert_ids * capacity + slots
    columns = jnp.arange(experts_all * capacity, dtype=jnp.int32)
    send_matrix = jnp.sum(
        (place[None, :, :] == columns[:, None, None]).astype(jnp.bfloat16), axis=2
    )
    take_matrix = jnp.sum(
        jnp.where(place[:, :, None] == columns[None, None, :], route_weight[:, :, None], 0.0),
        axis=1,
    )
    mixed_full = lax.all_gather(mixed, "tp", axis=1, tiled=True)
    normed2 = root_norm(mixed_full, ffn_gain).astype(jnp.bfloat16)
    dense_rows = lax.dynamic_slice_in_dim(normed2, tp_index * block_rows, block_rows, 0)
    outgoing = jnp.dot(send_matrix, normed2, preferred_element_type=jnp.float32).astype(
        jnp.bfloat16
    )
    outgoing = outgoing.reshape(experts_all, capacity, model_width)
    rows = lax.all_to_all(outgoing, "ep", split_axis=0, concat_axis=0, tiled=True)
    flat = rows.reshape(-1, rows.shape[2])
    gate_val = jnp.dot(flat, expert_gate[0], preferred_element_type=jnp.float32)
    up_val = jnp.dot(flat, expert_up[0], preferred_element_type=jnp.float32)
    inner = (jax.nn.silu(gate_val) * up_val).astype(jnp.bfloat16)
    partial_out = jnp.dot(inner, expert_down[0], preferred_element_type=jnp.float32).reshape(
        rows.shape
    )
    summed = lax.psum_scatter(
        partial_out.astype(jnp.bfloat16), "tp", scatter_dimension=2, tiled=True
    )
    returned = lax.all_to_all(summed, "ep", split_axis=0, concat_axis=0, tiled=True)
    moe_sum = jnp.dot(
        take_matrix,
        returned.reshape(-1, local_width).astype(jnp.float32),
        precision=lax.Precision.HIGHEST,
    )
    piece = lax.all_gather(dense_rows, "ep", axis=0, tiled=True)
    gate_val = jnp.dot(piece, dense_gate, preferred_element_type=jnp.float32)
    up_val = jnp.dot(piece, dense_up, preferred_element_type=jnp.float32)
    dense_hidden = (jax.nn.silu(gate_val) * up_val).astype(jnp.bfloat16)
    dense_own = lax.psum_scatter(
        jnp.dot(dense_hidden, dense_down, preferred_element_type=jnp.float32).astype(jnp.bfloat16),
        "ep",
        scatter_dimension=0,
        tiled=True,
    ).astype(jnp.float32)
    dense_out = lax.all_to_all(
        dense_own.astype(jnp.bfloat16), "tp", split_axis=1, concat_axis=0, tiled=True
    ).astype(dense_own.dtype)
    result = (
        mixed.astype(jnp.float32) + moe_sum + jax.nn.sigmoid(dense_mix)[None, :] * dense_out
    ).astype(jnp.bfloat16)
    return (result, new_state)


MESH = pl.DeviceIdType.MESH
F32 = jnp.float32
BF16 = jnp.bfloat16
GROUP = 8


def mm(left, right):
    return jnp.dot(left, right, preferred_element_type=F32)


def layer_kernel(
    dims,
    hidden,
    attn_gain,
    w_beta,
    w_decay,
    decay_scale,
    head_gain,
    ffn_gain,
    expert_ids,
    route_weight,
    dense_mix,
    state_hbm,
    wq_hbm,
    wk_hbm,
    wv_hbm,
    wg_hbm,
    wo_hbm,
    eg_hbm,
    eu_hbm,
    ed_hbm,
    dg_hbm,
    du_hbm,
    dd_hbm,
    out,
    state_out,
    st,
    wq,
    wk,
    wv,
    wg,
    wo,
    eg,
    eu,
    ed,
    dg,
    du,
    dd,
    x_all,
    q_s,
    k_s,
    v_s,
    g_s,
    b_s,
    d_s,
    read_s,
    heads_all,
    mixed_all,
    norm_s,
    piece_s,
    moe_rows,
    ids_all,
    dpart_send,
    dpart_recv,
    dfin_send,
    dfin_recv,
    inner_s,
    part_send,
    part_recv,
    own_s,
    pair_send,
    pair_recv,
    ret_send,
    ret_recv,
    load_sem,
    store_sem,
    tp_send,
    tp_recv,
    ep_send,
    ep_recv,
    fan_send,
    fan_recv,
):
    n_ep, n_tp, rows, lh, dk, cap = dims
    t = lax.axis_index("tp")
    e = lax.axis_index("ep")
    width = hidden.shape[1]
    block = rows // n_tp
    mate = t + 1 - 2 * lax.rem(t, 2)
    across = lax.rem(t + 2, n_tp)
    corner = lax.rem(mate + 2, n_tp)

    pairs = (
        (wq_hbm, wq),
        (wk_hbm, wk),
        (wv_hbm, wv),
        (wg_hbm, wg),
        (state_hbm, st),
        (wo_hbm, wo),
        (dg_hbm, dg),
        (du_hbm, du),
        (dd_hbm, dd),
        (eg_hbm.at[0], eg),
        (eu_hbm.at[0], eu),
        (ed_hbm.at[0], ed),
    )
    loads = [
        pltpu.make_async_copy(src, dst, load_sem.at[i]) for i, (src, dst) in enumerate(pairs)
    ]
    for load in loads[:5]:
        load.start()

    barrier = pltpu.get_barrier_semaphore()

    def greet_tp(i, carry):
        pl.semaphore_signal(
            barrier, inc=1, device_id={"tp": lax.rem(t + 1 + i, n_tp)}, device_id_type=MESH
        )
        return carry

    def greet_ep(i, carry):
        pl.semaphore_signal(
            barrier, inc=1, device_id={"ep": lax.rem(e + 1 + i, n_ep)}, device_id_type=MESH
        )
        return carry

    lax.fori_loop(0, n_tp - 1, greet_tp, 0)
    lax.fori_loop(0, n_ep - 1, greet_ep, 0)
    x_all[t] = hidden[...]
    ids_all[e] = jnp.zeros(ids_all.shape[1:], F32)
    ids_all[e, 0:2, 0:rows] = expert_ids[...].astype(F32)
    pl.semaphore_wait(barrier, n_tp + n_ep - 2)

    def tp_copy(phase, src, dst, i, peer):
        return pltpu.make_async_remote_copy(
            src_ref=src,
            dst_ref=dst,
            send_sem=tp_send.at[phase, i],
            recv_sem=tp_recv.at[phase, i],
            device_id={"tp": peer},
            device_id_type=MESH,
        )

    def ep_copy(phase, src, dst, i, peer):
        return pltpu.make_async_remote_copy(
            src_ref=src,
            dst_ref=dst,
            send_sem=ep_send.at[phase, i],
            recv_sem=ep_recv.at[phase, i],
            device_id={"ep": peer},
            device_id_type=MESH,
        )

    def exchange(make, phase, source, target, me, count):
        def send(i, carry):
            peer = lax.rem(me + 1 + i, count)
            make(phase, source(peer), target.at[me], i, peer).start()
            return carry

        lax.fori_loop(0, count - 1, send, 0)

    def arrive(make, phase, target, me, count):
        def take(i, carry):
            origin = lax.rem(me + count - 1 - i, count)
            make(phase, target.at[origin], target.at[origin], i, origin).wait_recv()
            return carry

        lax.fori_loop(0, count - 1, take, 0)

    def sent(make, phase, source, target, me, count):
        def leave(i, carry):
            peer = lax.rem(me + 1 + i, count)
            make(phase, source(peer), target.at[me], i, peer).wait_send()
            return carry

        lax.fori_loop(0, count - 1, leave, 0)

    exchange(tp_copy, 0, lambda p: x_all.at[t], x_all, t, n_tp)
    exchange(ep_copy, 0, lambda p: ids_all.at[e], ids_all, e, n_ep)
    for load in loads[5:]:
        load.start()
    arrive(tp_copy, 0, x_all, t, n_tp)

    def full_norm(chunks, gain_ref):
        wide = [chunk.astype(F32) for chunk in chunks]
        total = sum(jnp.sum(v * v, axis=-1, keepdims=True) for v in wide)
        scale = lax.rsqrt(total / (n_tp * width) + EPS)
        return jnp.concatenate(
            [wide[c] * scale * gain_ref[:, c * width : (c + 1) * width] for c in range(n_tp)],
            axis=1,
        )

    normed = full_norm([x_all[c] for c in range(n_tp)], attn_gain).astype(BF16)
    beta_all = lax.dot_general(
        normed, w_beta[...], (((1,), (1,)), ((), ())), preferred_element_type=F32
    )
    decay_all = lax.dot_general(
        normed, w_decay[...], (((1,), (1,)), ((), ())), preferred_element_type=F32
    )
    lane = lax.broadcasted_iota(jnp.int32, beta_all.shape, 1)
    lane_one = lax.broadcasted_iota(jnp.int32, decay_scale.shape, 1)
    for load in loads[:4]:
        load.wait()
    query_all = mm(normed, wq[...])
    key_all = mm(normed, wk[...])
    v_all = mm(normed, wv[...])
    g_all = mm(normed, wg[...])
    for h in range(lh):
        cut = slice(h * dk, (h + 1) * dk)
        head = t * lh + h
        q = query_all[:, cut]
        k = key_all[:, cut]
        q_s[h] = q * lax.rsqrt(jnp.sum(q * q, -1, keepdims=True) + EPS) * dk ** (-0.5)
        k_s[h] = k * lax.rsqrt(jnp.sum(k * k, -1, keepdims=True) + EPS)
        v_s[h] = v_all[:, cut]
        g_s[h] = g_all[:, cut]
        beta = jax.nn.sigmoid(
            jnp.sum(jnp.where(lane == head, beta_all, 0.0), -1, keepdims=True)
        )
        logit = jnp.sum(jnp.where(lane == head, decay_all, 0.0), -1, keepdims=True)
        rate = jnp.sum(jnp.where(lane_one == head, decay_scale[...], 0.0), -1, keepdims=True)
        soft = jnp.maximum(logit, 0.0) + jnp.log1p(jnp.exp(-jnp.abs(logit)))
        b_s[h] = jnp.broadcast_to(beta, (rows, dk))
        d_s[h] = jnp.broadcast_to(jnp.exp(-rate * soft), (rows, dk))

    loads[4].wait()

    def update(g, carry):
        start = pl.multiple_of(g * GROUP, GROUP)
        some = pl.ds(start, GROUP)
        for h in range(lh):
            k8 = k_s[h, some, :]
            q8 = q_s[h, some, :]
            v8 = v_s[h, some, :]
            b8 = b_s[h, some, :]
            d8 = d_s[h, some, :]
            kt = k8.T
            both = jnp.concatenate([k8, q8], axis=0).astype(BF16)
            qk = jnp.sum(q8 * k8, axis=-1, keepdims=True)
            reads = []
            for j in range(GROUP):
                old = st[start + j, h]
                rec = mm(both, old.astype(BF16))
                d = d8[j : j + 1]
                w = b8[j : j + 1] * (v8[j : j + 1] - d * rec[j : j + 1])
                st[start + j, h] = d * old + kt[:, j : j + 1] * w
                reads.append(d * rec[GROUP + j : GROUP + j + 1] + qk[j : j + 1] * w)
            read_s[h, some, :] = jnp.concatenate(reads, axis=0)
        return carry

    lax.fori_loop(0, rows // GROUP, update, 0)

    heads = []
    for h in range(lh):
        read = read_s[h]
        scale = lax.rsqrt(jnp.mean(read * read, -1, keepdims=True) + EPS)
        heads.append(read * scale * head_gain[...] * jax.nn.silu(g_s[h]))
    heads_all[t] = jnp.concatenate(heads, axis=1).astype(BF16)
    exchange(tp_copy, 1, lambda p: heads_all.at[t], heads_all, t, n_tp)
    state_copy = pltpu.make_async_copy(st, state_out, store_sem)
    state_copy.start()

    columns = n_ep * cap
    first = expert_ids[0:1, :]
    second = expert_ids[1:2, :]
    down_e = lax.broadcasted_iota(jnp.int32, (n_ep, rows), 0)
    hot0 = (down_e == first).astype(F32)
    hot1 = (down_e == second).astype(F32)
    later = (
        lax.broadcasted_iota(jnp.int32, (rows, rows), 0)
        < lax.broadcasted_iota(jnp.int32, (rows, rows), 1)
    ).astype(F32)
    later = later.astype(BF16)
    before = mm((hot0 + hot1).astype(BF16), later)
    slot0 = jnp.sum(before * hot0, 0, keepdims=True).astype(jnp.int32)
    slot1 = jnp.sum(before * hot1, 0, keepdims=True).astype(jnp.int32)
    down_c = lax.broadcasted_iota(jnp.int32, (columns, rows), 0)
    at0 = (down_c == first * cap + slot0).astype(F32)
    at1 = (down_c == second * cap + slot1).astype(F32)
    take_matrix = at0 * route_weight[0:1, :] + at1 * route_weight[1:2, :]

    arrive(tp_copy, 1, heads_all, t, n_tp)
    loads[5].wait()
    all_heads = jnp.concatenate([heads_all[c] for c in range(n_tp)], axis=1)
    mixed = (hidden[...].astype(F32) + mm(all_heads, wo[...])).astype(BF16)
    mixed_all[t, e] = mixed
    own_mixed = mixed_all.at[t]
    exchange(ep_copy, 1, lambda p: own_mixed.at[e], own_mixed, e, n_ep)

    def fan(kind, owner, s, peer):
        return pltpu.make_async_remote_copy(
            src_ref=mixed_all.at[owner, s],
            dst_ref=mixed_all.at[owner, s],
            send_sem=fan_send.at[kind, s],
            recv_sem=fan_recv.at[kind, s],
            device_id={"tp": peer},
            device_id_type=MESH,
        )

    fan(1, t, e, across).start()
    fan(0, t, e, mate).start()

    def forward(i, carry):
        s = lax.rem(e + n_ep - 1 - i, n_ep)
        ep_copy(1, own_mixed.at[s], own_mixed.at[s], i, s).wait_recv()
        fan(1, t, s, across).start()
        fan(0, t, s, mate).start()
        return carry

    lax.fori_loop(0, n_ep - 1, forward, 0)

    def relay(i, carry):
        s = lax.rem(e + n_ep - i, n_ep)
        fan(1, across, s, across).wait_recv()
        fan(2, across, s, mate).start()
        return carry

    lax.fori_loop(0, n_ep, relay, 0)
    arrive(ep_copy, 0, ids_all, e, n_ep)
    down_k = lax.broadcasted_iota(jnp.int32, (cap, rows), 0)
    wanted = e.astype(F32)

    def take_group(i, carry):
        s = lax.rem(e + n_ep - i, n_ep)
        hot = (ids_all[s] == wanted).astype(F32)[0:2, 0:rows]
        hot = hot[0:1] + hot[1:2]
        rank = mm(jnp.broadcast_to(hot, (8, rows)).astype(BF16), later)[0:1].astype(jnp.int32)
        pick = ((down_k == rank).astype(F32) * hot).astype(BF16)
        fan(0, mate, s, mate).wait_recv()
        fan(2, corner, s, mate).wait_recv()
        normed2 = full_norm([mixed_all[c, s] for c in range(n_tp)], ffn_gain)
        norm_s[...] = normed2
        piece_s[s] = norm_s[pl.ds(pl.multiple_of(t * block, block), block), :]
        moe_rows[s] = mm(pick, normed2.astype(BF16)).astype(BF16)
        return carry

    lax.fori_loop(0, n_ep, take_group, 0)

    for load in loads[6:9]:
        load.wait()
    piece = piece_s[...].reshape(n_ep * block, n_tp * width).astype(BF16)
    dense_hidden = (jax.nn.silu(mm(piece, dg[...])) * mm(piece, du[...])).astype(BF16)
    dense_cols = min(512, dd.shape[1])

    def dense_down(i, carry):
        cols = pl.ds(pl.multiple_of(i * dense_cols, dense_cols), dense_cols)
        value = mm(dense_hidden, dd[:, cols])
        dpart_send[:, :, cols] = value.reshape(n_ep, block, dense_cols).astype(BF16)
        return carry

    lax.fori_loop(0, dd.shape[1] // dense_cols, dense_down, 0)
    exchange(ep_copy, 2, lambda p: dpart_send.at[p], dpart_recv, e, n_ep)
    dpart_recv[e] = dpart_send[e]

    for load in loads[9:11]:
        load.wait()
    flat = moe_rows[...].reshape(n_ep * cap, n_tp * width)
    hidden_cols = 256

    def expert_inner(i, carry):
        cols = pl.ds(pl.multiple_of(i * hidden_cols, hidden_cols), hidden_cols)
        inner_s[:, cols] = (
            jax.nn.silu(mm(flat, eg[:, cols])) * mm(flat, eu[:, cols])
        ).astype(BF16)
        return carry

    lax.fori_loop(0, eg.shape[1] // hidden_cols, expert_inner, 0)
    loads[11].wait()

    def expert_down(chunk):
        cols = pl.ds(pl.multiple_of(chunk * width, width), width)
        return mm(inner_s[...], ed[:, cols])

    def to_mate(i):
        return pltpu.make_async_remote_copy(
            src_ref=part_send.at[i],
            dst_ref=part_recv.at[i],
            send_sem=tp_send.at[2, i],
            recv_sem=tp_recv.at[2, i],
            device_id={"tp": mate},
            device_id_type=MESH,
        )

    def to_mate_step(i, carry):
        part_send[i] = expert_down(lax.rem(mate + 2 - 2 * i, n_tp)).astype(BF16)
        to_mate(i).start()
        return carry

    lax.fori_loop(0, 2, to_mate_step, 0)
    pair = pltpu.make_async_remote_copy(
        src_ref=pair_send,
        dst_ref=pair_recv,
        send_sem=tp_send.at[3, 0],
        recv_sem=tp_recv.at[3, 0],
        device_id={"tp": across},
        device_id_type=MESH,
    )

    def own_step(i, carry):
        value = expert_down(lax.rem(t + 2 - 2 * i, n_tp))
        to_mate(i).wait_recv()
        own_s[i] = value + part_recv[i].astype(F32)

        @pl.when(i == 0)
        def _():
            pair_send[...] = own_s[0].astype(BF16)
            pair.start()

        return carry

    lax.fori_loop(0, 2, own_step, 0)

    arrive(ep_copy, 2, dpart_recv, e, n_ep)
    dense_own = sum(dpart_recv[c].astype(F32) for c in range(n_ep))
    for c in range(n_tp):
        dfin_send[c] = dense_own[:, c * width : (c + 1) * width].astype(BF16)
    exchange(tp_copy, 4, lambda p: dfin_send.at[p], dfin_recv, t, n_tp)
    dfin_recv[t] = dfin_send[t]

    pair.wait_recv()
    summed = (own_s[1] + pair_recv[...].astype(F32)).astype(BF16)
    ret_send[...] = summed.reshape(ret_send.shape)
    exchange(ep_copy, 3, lambda p: ret_send.at[p], ret_recv, e, n_ep)
    ret_recv[e] = ret_send[e]
    arrive(tp_copy, 4, dfin_recv, t, n_tp)
    dense_out = dfin_recv[...].astype(F32).reshape(rows, width)
    base = mixed.astype(F32) + jax.nn.sigmoid(dense_mix[...]) * dense_out
    high = take_matrix.astype(BF16)
    low = (take_matrix - high.astype(F32)).astype(BF16)
    arrive(ep_copy, 3, ret_recv, e, n_ep)
    returned = ret_recv[...].reshape(columns, width)
    over = (((0,), (0,)), ((), ()))
    moe_sum = lax.dot_general(
        high, returned, over, preferred_element_type=F32
    ) + lax.dot_general(low, returned, over, preferred_element_type=F32)
    out[...] = (base + moe_sum).astype(BF16)

    sent(tp_copy, 0, lambda p: x_all.at[t], x_all, t, n_tp)
    sent(tp_copy, 1, lambda p: heads_all.at[t], heads_all, t, n_tp)
    sent(tp_copy, 4, lambda p: dfin_send.at[p], dfin_recv, t, n_tp)
    sent(ep_copy, 0, lambda p: ids_all.at[e], ids_all, e, n_ep)
    sent(ep_copy, 1, lambda p: own_mixed.at[e], own_mixed, e, n_ep)
    sent(ep_copy, 2, lambda p: dpart_send.at[p], dpart_recv, e, n_ep)
    sent(ep_copy, 3, lambda p: ret_send.at[p], ret_recv, e, n_ep)
    pair.wait_send()

    def sent_mate(i, carry):
        to_mate(i).wait_send()
        return carry

    lax.fori_loop(0, 2, sent_mate, 0)

    def sent_fan(s, carry):
        fan(0, t, s, mate).wait_send()
        fan(1, t, s, across).wait_send()
        fan(2, across, s, mate).wait_send()
        return carry

    lax.fori_loop(0, n_ep, sent_fan, 0)
    state_copy.wait()


def fused_device(n_ep, n_tp, *args):
    (
        hidden_in,
        state_in,
        attn_gain,
        w_query,
        w_key,
        w_value,
        w_gate,
        w_beta,
        w_decay,
        decay_scale,
        head_gain,
        w_output,
        ffn_gain,
        expert_ids,
        route_weight,
        expert_gate,
        expert_up,
        expert_down,
        dense_gate,
        dense_up,
        dense_down,
        dense_mix,
    ) = args
    rows, width = hidden_in.shape
    lh, dk, dv = state_in.shape[1:]
    cap = max(2, 2 * rows * expert_ids.shape[1] // n_ep)
    block = rows // n_tp
    model = width * n_tp
    vmem = pltpu.VMEM
    whole = pl.BlockSpec(memory_space=pltpu.VMEM)
    away = pl.BlockSpec(memory_space=pl.ANY)
    head_shape = (lh, rows, dk)

    def like(array):
        return vmem(array.shape, array.dtype)

    scratch = [
        like(state_in),
        like(w_query),
        like(w_key),
        like(w_value),
        like(w_gate),
        like(w_output),
        vmem(expert_gate.shape[1:], BF16),
        vmem(expert_up.shape[1:], BF16),
        vmem(expert_down.shape[1:], BF16),
        like(dense_gate),
        like(dense_up),
        like(dense_down),
        vmem((n_tp, rows, width), BF16),
        *[vmem(head_shape, F32) for _ in range(7)],
        vmem((n_tp, rows, lh * dv), BF16),
        vmem((n_tp, n_ep, rows, width), BF16),
        vmem((rows, model), F32),
        vmem((n_ep, block, model), F32),
        vmem((n_ep, cap, model), BF16),
        vmem((n_ep, 8, 128), F32),
        vmem((n_ep, block, model), BF16),
        vmem((n_ep, block, model), BF16),
        vmem((n_tp, block, width), BF16),
        vmem((n_tp, block, width), BF16),
        vmem((n_ep * cap, expert_gate.shape[2]), BF16),
        vmem((2, n_ep * cap, width), BF16),
        vmem((2, n_ep * cap, width), BF16),
        vmem((2, n_ep * cap, width), F32),
        vmem((n_ep * cap, width), BF16),
        vmem((n_ep * cap, width), BF16),
        vmem((n_ep, cap, width), BF16),
        vmem((n_ep, cap, width), BF16),
        pltpu.SemaphoreType.DMA((12,)),
        pltpu.SemaphoreType.DMA,
        pltpu.SemaphoreType.DMA((5, n_tp - 1)),
        pltpu.SemaphoreType.DMA((5, n_tp - 1)),
        pltpu.SemaphoreType.DMA((4, n_ep - 1)),
        pltpu.SemaphoreType.DMA((4, n_ep - 1)),
        pltpu.SemaphoreType.DMA((3, n_ep)),
        pltpu.SemaphoreType.DMA((3, n_ep)),
    ]
    return tuple(
        pl.pallas_call(
            functools.partial(layer_kernel, (n_ep, n_tp, rows, lh, dk, cap)),
            out_shape=(
                jax.ShapeDtypeStruct(hidden_in.shape, BF16),
                jax.ShapeDtypeStruct(state_in.shape, F32),
            ),
            in_specs=[whole] * 10 + [away] * 12,
            out_specs=(whole, away),
            scratch_shapes=scratch,
            compiler_params=pltpu.CompilerParams(
                collective_id=0, has_side_effects=True, vmem_limit_bytes=60 * 1024 * 1024
            ),
        )(
            hidden_in,
            attn_gain.reshape(1, -1),
            w_beta.T,
            w_decay.T,
            decay_scale.reshape(1, -1),
            head_gain.reshape(1, -1),
            ffn_gain.reshape(1, -1),
            expert_ids.T,
            route_weight.T,
            dense_mix.reshape(1, -1),
            state_in,
            w_query,
            w_key,
            w_value,
            w_gate,
            w_output,
            expert_gate,
            expert_up,
            expert_down,
            dense_gate,
            dense_up,
            dense_down,
        )
    )


def device_program(n_ep, n_tp, *args):
    rows, width = args[0].shape
    top = args[13].shape[1]
    cap = max(2, 2 * rows * top // n_ep)
    fits = (
        top == 2
        and n_tp == 4
        and rows <= 128
        and args[15].shape[0] == 1
        and cap % 16 == 0
        and rows % GROUP == 0
        and (rows // n_tp) % 8 == 0
        and width % 128 == 0
        and args[15].shape[2] % 256 == 0
        and n_ep <= 128
    )
    if fits:
        return fused_device(n_ep, n_tp, *args)
    return per_device(*args)


def solution(mesh):
    placed = (
        P("ep", "tp"),
        P("ep", "tp", None, None),
        P(),
        P(None, "tp"),
        P(None, "tp"),
        P(None, "tp"),
        P(None, "tp"),
        P(),
        P(),
        P(),
        P(),
        P(None, "tp"),
        P(),
        P("ep", None),
        P("ep", None),
        P("ep", None, "tp"),
        P("ep", None, "tp"),
        P("ep", "tp", None),
        P(None, "ep"),
        P(None, "ep"),
        P("ep", None),
        P("tp"),
    )
    return jax.shard_map(
        functools.partial(device_program, mesh.shape["ep"], mesh.shape["tp"]),
        mesh=mesh,
        in_specs=placed,
        out_specs=(P("ep", "tp"), P("ep", "tp", None, None)),
        check_vma=False,
    )
```

profile of v0, /device:TPU:0, one launch (start us, length us, event | category | flops | bytes accessed | tf_op | source)
XLA Modules:
  0.0 54.0 jit_solution(11754778149084425210)
XLA Ops:
  0.6 47.3 %shard_map.221 = (bf16[32,512]{1,0:T(8,128)(2,1)}, f32[32,2,128,128]{3,2,1,0:T(8,128)}) custom-call(bf16[32,512]{1,0:T(8,128)(2,1)} %hidden.1, f32[1,2048]{1,0:T(1,128)} %bitcast.11, bf16[8,2048]{1,0:T(8,128)(2,1)} %bitcast.9, bf16[8,2048]{1,0:T(8,128)(2,1)} %bitcast.10, f32[1,8]{1,0:T(1,128)} %bitcast.16, f32[1,128]{1,0:T(1,128)} %bitcast.17, ...), custom_call_target="tpu_custom_call" | custom-call | tf_op jit(solution)/shard_map/pallas_call | solution.py:710
  48.0 1.4 %copy.26 = bf16[32,512]{1,0:T(8,128)(2,1)} copy(bf16[32,512]{1,0:T(8,128)(2,1)} %get-tuple-element.4) | data formatting | bytes 65536
  49.3 4.7 %copy.27 = f32[32,2,128,128]{3,2,1,0:T(8,128)} copy(f32[32,2,128,128]{3,2,1,0:T(8,128)} %get-tuple-element.5) | data formatting | bytes 8388608
where the time goes:
time: 54.3 us; the launch traced here: 54 us
  Pallas kernels  47.3 us (87%)
  local copies, waits for them, and re-layouts  6.07 us (11%)
  between operations  0.65 us (1%)
    pallas_call x1, Pallas kernels, fused_device(): pl.pallas_call(functools.partial(layer_kernel, (n_ep, n_tp, rows, lh, dk,...  47.3 us
    unnamed x2, local copies, waits for them, and re-layouts  6.07 us

commit v1 on v0

--- a/solution.py
+++ b/solution.py
@@ -199,7 +199,6 @@
     du_hbm,
     dd_hbm,
     out,
-    state_out,
     st,
     wq,
     wk,
@@ -239,7 +238,6 @@
     ret_send,
     ret_recv,
     load_sem,
-    store_sem,
     tp_send,
     tp_recv,
     ep_send,
@@ -423,8 +421,6 @@
         heads.append(read * scale * head_gain[...] * jax.nn.silu(g_s[h]))
     heads_all[t] = jnp.concatenate(heads, axis=1).astype(BF16)
     exchange(tp_copy, 1, lambda p: heads_all.at[t], heads_all, t, n_tp)
-    state_copy = pltpu.make_async_copy(st, state_out, store_sem)
-    state_copy.start()
 
     columns = n_ep * cap
     first = expert_ids[0:1, :]
@@ -623,7 +619,34 @@
         return carry
 
     lax.fori_loop(0, n_ep, sent_fan, 0)
-    state_copy.wait()
+
+
+def store_kernel(res, state, out, state_out, sem):
+    copies = [
+        pltpu.make_async_copy(res, out, sem.at[0]),
+        pltpu.make_async_copy(state, state_out, sem.at[1]),
+    ]
+    for copy in copies:
+        copy.start()
+    for copy in copies:
+        copy.wait()
+
+
+def store_outputs(res, state):
+    away = pl.BlockSpec(memory_space=pl.ANY)
+    return tuple(
+        pl.pallas_call(
+            store_kernel,
+            out_shape=(
+                jax.ShapeDtypeStruct(res.shape, res.dtype),
+                jax.ShapeDtypeStruct(state.shape, state.dtype),
+            ),
+            in_specs=[away, away],
+            out_specs=(away, away),
+            scratch_shapes=[pltpu.SemaphoreType.DMA((2,))],
+            compiler_params=pltpu.CompilerParams(vmem_limit_bytes=1024 * 1024),
+        )(res, state)
+    )
 
 
 def fused_device(n_ep, n_tp, *args):
@@ -665,7 +688,6 @@
         return vmem(array.shape, array.dtype)
 
     scratch = [
-        like(state_in),
         like(w_query),
         like(w_key),
         like(w_value),
@@ -698,7 +720,6 @@
         vmem((n_ep, cap, width), BF16),
         vmem((n_ep, cap, width), BF16),
         pltpu.SemaphoreType.DMA((12,)),
-        pltpu.SemaphoreType.DMA,
         pltpu.SemaphoreType.DMA((5, n_tp - 1)),
         pltpu.SemaphoreType.DMA((5, n_tp - 1)),
         pltpu.SemaphoreType.DMA((4, n_ep - 1)),
@@ -706,18 +727,18 @@
         pltpu.SemaphoreType.DMA((3, n_ep)),
         pltpu.SemaphoreType.DMA((3, n_ep)),
     ]
-    return tuple(
-        pl.pallas_call(
+    return store_outputs(
+        *pl.pallas_call(
             functools.partial(layer_kernel, (n_ep, n_tp, rows, lh, dk, cap)),
             out_shape=(
-                jax.ShapeDtypeStruct(hidden_in.shape, BF16),
-                jax.ShapeDtypeStruct(state_in.shape, F32),
+                pltpu.VMEM(hidden_in.shape, BF16),
+                pltpu.VMEM(state_in.shape, F32),
             ),
             in_specs=[whole] * 10 + [away] * 12,
-            out_specs=(whole, away),
+            out_specs=(whole, whole),
             scratch_shapes=scratch,
             compiler_params=pltpu.CompilerParams(
-                collective_id=0, has_side_effects=True, vmem_limit_bytes=60 * 1024 * 1024
+                collective_id=0, has_side_effects=True, vmem_limit_bytes=58 * 1024 * 1024
             ),
         )(
             hidden_in,

time: 54.3 us -> 49.5 us (0.912)
  local copies, waits for them, and re-layouts: 6.07 us -> 0 us
  Pallas kernels: 47.3 us -> 48.7 us
    unnamed x2 -> x0, local copies, waits for them, and re-layouts: 6.07 us -> none
    pallas_call x0 -> x1, Pallas kernels: none -> 2.04 us  [store_outputs(): pl.pallas_call(store_kernel, out_shape=(jax.ShapeDtypeStruct(res.shape, r...]
    pallas_call x1, Pallas kernels: 47.3 us -> 46.7 us  [fused_device(): pl.pallas_call(functools.partial(layer_kernel, (n_ep, n_tp, rows, lh, dk,...]
where the time goes in v1:
time: 49.5 us; the launch traced here: 49.4 us
  Pallas kernels  48.7 us (98%)
  between operations  0.65 us (1%)
    pallas_call x1, Pallas kernels, fused_device(): pl.pallas_call(functools.partial(layer_kernel, (n_ep, n_tp, rows, lh, dk,...  46.7 us
    pallas_call x1, Pallas kernels, store_outputs(): pl.pallas_call(store_kernel, out_shape=(jax.ShapeDtypeStruct(res.shape, r...  2.04 us

profile of v1, /device:TPU:0, one launch (start us, length us, event | category | flops | bytes accessed | tf_op | source)
XLA Modules:
  0.0 49.4 jit_solution(8826040362273129515)
XLA Ops:
  0.6 46.7 %shard_map.221 = (bf16[32,512]{1,0:T(8,128)(2,1)S(1)}, f32[32,2,128,128]{3,2,1,0:T(8,128)S(1)}) custom-call(bf16[32,512]{1,0:T(8,128)(2,1)} %hidden.1, f32[1,2048]{1,0:T(1,128)} %bitcast.11, bf16[8,2048]{1,0:T(8,128)(2,1)} %bitcast.9, bf16[8,2048]{1,0:T(8,128)(2,1)} %bitcast.10, f32[1,8]{1,0:T(1,128)} %bitcast.16, f32[1,128]{1,0:T(1,128)} %bitcast.17, ...), custom_call_target="tpu_custom_call" | custom-call | tf_op jit(solution)/shard_map/pallas_call | solution.py:731
  47.3 2.0 %shard_map.222 = (bf16[32,512]{1,0:T(8,128)(2,1)}, f32[32,2,128,128]{3,2,1,0:T(8,128)}) custom-call(bf16[32,512]{1,0:T(8,128)(2,1)S(1)} %get-tuple-element.4.res, f32[32,2,128,128]{3,2,1,0:T(8,128)S(1)} %get-tuple-element.5.state), custom_call_target="tpu_custom_call" | custom-call | tf_op jit(solution)/shard_map/pallas_call | solution.py:638

commit v2 on v1

--- a/solution.py
+++ b/solution.py
@@ -176,16 +176,16 @@
 
 def layer_kernel(
     dims,
-    hidden,
-    attn_gain,
-    w_beta,
-    w_decay,
-    decay_scale,
-    head_gain,
-    ffn_gain,
-    expert_ids,
-    route_weight,
-    dense_mix,
+    hidden_hbm,
+    again_hbm,
+    w_beta_hbm,
+    w_decay_hbm,
+    decay_scale_hbm,
+    head_gain_hbm,
+    fgain_hbm,
+    ids_hbm,
+    rweight_hbm,
+    dmix_hbm,
     state_hbm,
     wq_hbm,
     wk_hbm,
@@ -200,6 +200,15 @@
     dd_hbm,
     out,
     st,
+    attn_gain,
+    w_beta,
+    w_decay,
+    decay_scale,
+    head_gain,
+    ffn_gain,
+    expert_ids,
+    route_weight,
+    dense_mix,
     wq,
     wk,
     wv,
@@ -221,9 +230,9 @@
     read_s,
     heads_all,
     mixed_all,
-    norm_s,
     piece_s,
     moe_rows,
+    pick_s,
     ids_all,
     dpart_send,
     dpart_recv,
@@ -237,23 +246,54 @@
     pair_recv,
     ret_send,
     ret_recv,
+    small_sem,
     load_sem,
     tp_send,
     tp_recv,
     ep_send,
     ep_recv,
-    fan_send,
-    fan_recv,
+    line_send,
+    side_send,
+    across_send,
+    mate_send,
+    block_recv,
+    dense_send,
+    dense_recv,
+    give_recv,
+    token,
 ):
     n_ep, n_tp, rows, lh, dk, cap = dims
     t = lax.axis_index("tp")
     e = lax.axis_index("ep")
-    width = hidden.shape[1]
+    width = x_all.shape[2]
     block = rows // n_tp
     mate = t + 1 - 2 * lax.rem(t, 2)
     across = lax.rem(t + 2, n_tp)
     corner = lax.rem(mate + 2, n_tp)
-
+    last = n_ep // 2 - 1
+    z = e // 2
+    x = e - 2 * z
+    beside = 2 * z + 1 - x
+    near = (z, z + 1 - 2 * lax.rem(z, 2), 2 - z // 2, last * (1 - z // 2))
+    at_end = z * (last - z) == 0
+
+    smalls = [
+        pltpu.make_async_copy(src, dst, small_sem.at[i])
+        for i, (src, dst) in enumerate(
+            (
+                (hidden_hbm, x_all.at[t]),
+                (again_hbm, attn_gain),
+                (w_beta_hbm, w_beta),
+                (w_decay_hbm, w_decay),
+                (decay_scale_hbm, decay_scale),
+                (ids_hbm, expert_ids),
+                (head_gain_hbm, head_gain),
+                (fgain_hbm, ffn_gain),
+                (rweight_hbm, route_weight),
+                (dmix_hbm, dense_mix),
+            )
+        )
+    ]
     pairs = (
         (wq_hbm, wq),
         (wk_hbm, wk),
@@ -271,9 +311,6 @@
     loads = [
         pltpu.make_async_copy(src, dst, load_sem.at[i]) for i, (src, dst) in enumerate(pairs)
     ]
-    for load in loads[:5]:
-        load.start()
-
     barrier = pltpu.get_barrier_semaphore()
 
     def greet_tp(i, carry):
@@ -282,18 +319,29 @@
         )
         return carry
 
-    def greet_ep(i, carry):
-        pl.semaphore_signal(
-            barrier, inc=1, device_id={"ep": lax.rem(e + 1 + i, n_ep)}, device_id_type=MESH
-        )
-        return carry
-
+    def greet(sem, place):
+        pl.semaphore_signal(sem, inc=1, device_id={"ep": place}, device_id_type=MESH)
+
+    smalls[0].start()
     lax.fori_loop(0, n_tp - 1, greet_tp, 0)
-    lax.fori_loop(0, n_ep - 1, greet_ep, 0)
-    x_all[t] = hidden[...]
-    ids_all[e] = jnp.zeros(ids_all.shape[1:], F32)
-    ids_all[e, 0:2, 0:rows] = expert_ids[...].astype(F32)
-    pl.semaphore_wait(barrier, n_tp + n_ep - 2)
+    greet(barrier, beside)
+
+    @pl.when(z > 0)
+    def _():
+        greet(barrier, e - 2)
+
+    @pl.when(z < last)
+    def _():
+        greet(barrier, e + 2)
+
+    for load in smalls[1:]:
+        load.start()
+    for load in loads[:5]:
+        load.start()
+    smalls[0].wait()
+
+    ends = (z + last - 1) // last + (2 * last - z - 1) // last
+    pl.semaphore_wait(barrier, n_tp + ends)
 
     def tp_copy(phase, src, dst, i, peer):
         return pltpu.make_async_remote_copy(
@@ -339,36 +387,89 @@
 
         lax.fori_loop(0, count - 1, leave, 0)
 
-    exchange(tp_copy, 0, lambda p: x_all.at[t], x_all, t, n_tp)
-    exchange(ep_copy, 0, lambda p: ids_all.at[e], ids_all, e, n_ep)
+    def tp_move(phase, buffer, owner, peer, kind):
+        return pltpu.make_async_remote_copy(
+            src_ref=buffer.at[owner],
+            dst_ref=buffer.at[owner],
+            send_sem=tp_send.at[phase, kind],
+            recv_sem=tp_recv.at[phase, kind],
+            device_id={"tp": peer},
+            device_id_type=MESH,
+        )
+
+    others = (mate, across, corner)
+
+    def tp_share(phase, buffer):
+        for kind in (1, 2, 0):
+            tp_move(phase, buffer, t, others[kind], kind).start()
+
+    def tp_take(phase, buffer, kind):
+        tp_move(phase, buffer, others[kind], others[kind], kind).wait_recv()
+
+    def tp_left(phase, buffer):
+        for kind in range(3):
+            tp_move(phase, buffer, t, others[kind], kind).wait_send()
+
+    tp_share(0, x_all)
     for load in loads[5:]:
         load.start()
-    arrive(tp_copy, 0, x_all, t, n_tp)
-
-    def full_norm(chunks, gain_ref):
-        wide = [chunk.astype(F32) for chunk in chunks]
-        total = sum(jnp.sum(v * v, axis=-1, keepdims=True) for v in wide)
-        scale = lax.rsqrt(total / (n_tp * width) + EPS)
-        return jnp.concatenate(
-            [wide[c] * scale * gain_ref[:, c * width : (c + 1) * width] for c in range(n_tp)],
-            axis=1,
-        )
-
-    normed = full_norm([x_all[c] for c in range(n_tp)], attn_gain).astype(BF16)
-    beta_all = lax.dot_general(
-        normed, w_beta[...], (((1,), (1,)), ((), ())), preferred_element_type=F32
-    )
-    decay_all = lax.dot_general(
-        normed, w_decay[...], (((1,), (1,)), ((), ())), preferred_element_type=F32
-    )
+
+    @pl.when(z == 1)
+    def _():
+        greet(token.at[0], e + 2)
+
+    @pl.when(z == last - 1)
+    def _():
+        greet(token.at[1], e - 2)
+
+    for load in smalls[1:]:
+        load.wait()
+    for load in loads[:4]:
+        load.wait()
+    ids_all[e] = jnp.zeros(ids_all.shape[1:], F32)
+    ids_all[e, 0:2, 0:rows] = expert_ids[...].astype(F32)
+
+    def project(owner):
+        cols = pl.ds(pl.multiple_of(owner * width, width), width)
+        wide = x_all[owner].astype(F32)
+        total = jnp.sum(wide * wide, axis=-1, keepdims=True)
+        part = (wide * attn_gain[:, cols]).astype(BF16)
+        over = (((1,), (1,)), ((), ()))
+        return (
+            total,
+            mm(part, wq[cols, :]),
+            mm(part, wk[cols, :]),
+            mm(part, wv[cols, :]),
+            mm(part, wg[cols, :]),
+            lax.dot_general(part, w_beta[:, cols], over, preferred_element_type=F32),
+            lax.dot_general(part, w_decay[:, cols], over, preferred_element_type=F32),
+        )
+
+    def plus(left, right):
+        return tuple(a + b for a, b in zip(left, right))
+
+    sums = project(t)
+    tp_take(0, x_all, 0)
+    sums = plus(sums, project(mate))
+    tp_take(0, x_all, 1)
+    sums = plus(sums, project(across))
+    tp_take(0, x_all, 2)
+    sums = plus(sums, project(corner))
+
+    @pl.when(z == 2)
+    def _():
+        pl.semaphore_wait(token.at[0], 1)
+        greet(token.at[0], e + 2)
+
+    @pl.when(z == last - 2)
+    def _():
+        pl.semaphore_wait(token.at[1], 1)
+        greet(token.at[1], e - 2)
+
+    scale = lax.rsqrt(sums[0] / (n_tp * width) + EPS)
+    query_all, key_all, v_all, g_all, beta_all, decay_all = [v * scale for v in sums[1:]]
     lane = lax.broadcasted_iota(jnp.int32, beta_all.shape, 1)
     lane_one = lax.broadcasted_iota(jnp.int32, decay_scale.shape, 1)
-    for load in loads[:4]:
-        load.wait()
-    query_all = mm(normed, wq[...])
-    key_all = mm(normed, wk[...])
-    v_all = mm(normed, wv[...])
-    g_all = mm(normed, wg[...])
     for h in range(lh):
         cut = slice(h * dk, (h + 1) * dk)
         head = t * lh + h
@@ -389,30 +490,32 @@
 
     loads[4].wait()
 
-    def update(g, carry):
+    sub = lax.broadcasted_iota(jnp.int32, (GROUP, dk), 0)
+
+    def recall(g, carry):
         start = pl.multiple_of(g * GROUP, GROUP)
         some = pl.ds(start, GROUP)
         for h in range(lh):
             k8 = k_s[h, some, :]
             q8 = q_s[h, some, :]
-            v8 = v_s[h, some, :]
-            b8 = b_s[h, some, :]
             d8 = d_s[h, some, :]
-            kt = k8.T
             both = jnp.concatenate([k8, q8], axis=0).astype(BF16)
+            rec_k = jnp.zeros((GROUP, dk), F32)
+            rec_q = jnp.zeros((GROUP, dk), F32)
+            for j in range(0, GROUP, 2):
+                two = jnp.concatenate([st[start + j, h], st[start + j + 1, h]], axis=1)
+                rec = mm(both, two.astype(BF16))
+                for i in range(2):
+                    part = rec[:, i * dk : (i + 1) * dk]
+                    rec_k = jnp.where(sub == j + i, part[:GROUP], rec_k)
+                    rec_q = jnp.where(sub == j + i, part[GROUP:], rec_q)
+            w8 = b_s[h, some, :] * (v_s[h, some, :] - d8 * rec_k)
+            v_s[h, some, :] = w8
             qk = jnp.sum(q8 * k8, axis=-1, keepdims=True)
-            reads = []
-            for j in range(GROUP):
-                old = st[start + j, h]
-                rec = mm(both, old.astype(BF16))
-                d = d8[j : j + 1]
-                w = b8[j : j + 1] * (v8[j : j + 1] - d * rec[j : j + 1])
-                st[start + j, h] = d * old + kt[:, j : j + 1] * w
-                reads.append(d * rec[GROUP + j : GROUP + j + 1] + qk[j : j + 1] * w)
-            read_s[h, some, :] = jnp.concatenate(reads, axis=0)
+            read_s[h, some, :] = d8 * rec_q + qk * w8
         return carry
 
-    lax.fori_loop(0, rows // GROUP, update, 0)
+    lax.fori_loop(0, rows // GROUP, recall, 0)
 
     heads = []
     for h in range(lh):
@@ -420,8 +523,130 @@
         scale = lax.rsqrt(jnp.mean(read * read, -1, keepdims=True) + EPS)
         heads.append(read * scale * head_gain[...] * jax.nn.silu(g_s[h]))
     heads_all[t] = jnp.concatenate(heads, axis=1).astype(BF16)
-    exchange(tp_copy, 1, lambda p: heads_all.at[t], heads_all, t, n_tp)
-
+    tp_share(1, heads_all)
+
+    @pl.when(z == last)
+    def _():
+        pl.semaphore_wait(token.at[0], 1)
+
+    @pl.when(z == 0)
+    def _():
+        pl.semaphore_wait(token.at[1], 1)
+
+    greet(token.at[2], beside)
+
+    def rank_one(g, carry):
+        start = pl.multiple_of(g * GROUP, GROUP)
+        some = pl.ds(start, GROUP)
+        for h in range(lh):
+            kt = k_s[h, some, :].T
+            w8 = v_s[h, some, :]
+            d8 = d_s[h, some, :]
+            for j in range(GROUP):
+                st[start + j, h] = d8[j : j + 1] * st[start + j, h] + kt[:, j : j + 1] * w8[j : j + 1]
+        return carry
+
+    groups = rows // GROUP
+    lax.fori_loop(0, groups // 2, rank_one, 0)
+    pl.semaphore_wait(token.at[2], 1)
+    exchange(ep_copy, 0, lambda p: ids_all.at[e], ids_all, e, n_ep)
+    lax.fori_loop(groups // 2, groups - 1, rank_one, 0)
+    loads[5].wait()
+    head_cols = heads_all.shape[2]
+
+    def wo_part(owner):
+        return mm(heads_all[owner], wo[pl.ds(pl.multiple_of(owner * head_cols, head_cols), head_cols), :])
+
+    mixed = x_all[t].astype(F32) + wo_part(t)
+    tp_take(1, heads_all, 0)
+    mixed = mixed + wo_part(mate)
+    tp_take(1, heads_all, 1)
+    mixed = mixed + wo_part(across)
+    tp_take(1, heads_all, 2)
+    mixed = (mixed + wo_part(corner)).astype(BF16)
+    mixed_all[t, e] = mixed
+
+    def move(owner, s, sem, place):
+        return pltpu.make_async_remote_copy(
+            src_ref=mixed_all.at[owner, s],
+            dst_ref=mixed_all.at[owner, s],
+            send_sem=sem,
+            recv_sem=block_recv.at[owner, s],
+            device_id=place,
+            device_id_type=MESH,
+        )
+
+    def here(k, side):
+        return 2 * near[k] + (x if side == 0 else 1 - x)
+
+    def along(k):
+        return move(t, e, line_send.at[k - 1], {"ep": here(k, 0)})
+
+    def far():
+        return move(t, e, line_send.at[3], {"ep": here(3, 1)})
+
+    def aside(k):
+        return move(t, here(k, 0), side_send.at[k], {"ep": beside})
+
+    def over_y(k, side):
+        return move(t, here(k, side), across_send.at[k, side], {"tp": across})
+
+    def to_core(k, side, owner, i):
+        return move(owner, here(k, side), mate_send.at[i, k, side], {"tp": mate})
+
+    def spread(k, side):
+        over_y(k, side).start()
+        to_core(k, side, t, 0).start()
+
+    def got(k, side, owner):
+        s = here(k, side)
+        move(owner, s, mate_send.at[0, k, side], {"tp": mate}).wait_recv()
+
+    def from_line(k):
+        got(k, 0, t)
+        if k < 3:
+            aside(k).start()
+        else:
+
+            @pl.when(jnp.logical_not(at_end))
+            def _():
+                aside(k).start()
+
+        spread(k, 0)
+
+    def from_side(k):
+        got(k, 1, t)
+        spread(k, 1)
+
+    def from_across(k, side):
+        got(k, side, across)
+        to_core(k, side, across, 1).start()
+
+    def take_group(k, side):
+        s = here(k, side)
+        got(k, side, mate)
+        got(k, side, corner)
+        pick = pick_s[s].astype(BF16)
+        wide = [mm(pick, mixed_all[c, s]) for c in range(n_tp)]
+        total = sum(jnp.sum(v * v, axis=-1, keepdims=True) for v in wide)
+        scale = lax.rsqrt(total / (n_tp * width) + EPS)
+        for c in range(n_tp):
+            cols = slice(c * width, (c + 1) * width)
+            value = wide[c] * scale * ffn_gain[:, cols]
+            moe_rows[2 * k + side, :, cols] = value[:cap].astype(BF16)
+            piece_s[2 * k + side, :, cols] = value[cap:]
+
+    along(3).start()
+
+    @pl.when(at_end)
+    def _():
+        far().start()
+
+    spread(0, 0)
+    aside(0).start()
+    along(2).start()
+    along(1).start()
+    lax.fori_loop(groups - 1, groups, rank_one, 0)
     columns = n_ep * cap
     first = expert_ids[0:1, :]
     second = expert_ids[1:2, :]
@@ -441,78 +666,80 @@
     at1 = (down_c == second * cap + slot1).astype(F32)
     take_matrix = at0 * route_weight[0:1, :] + at1 * route_weight[1:2, :]
 
-    arrive(tp_copy, 1, heads_all, t, n_tp)
-    loads[5].wait()
-    all_heads = jnp.concatenate([heads_all[c] for c in range(n_tp)], axis=1)
-    mixed = (hidden[...].astype(F32) + mm(all_heads, wo[...])).astype(BF16)
-    mixed_all[t, e] = mixed
-    own_mixed = mixed_all.at[t]
-    exchange(ep_copy, 1, lambda p: own_mixed.at[e], own_mixed, e, n_ep)
-
-    def fan(kind, owner, s, peer):
-        return pltpu.make_async_remote_copy(
-            src_ref=mixed_all.at[owner, s],
-            dst_ref=mixed_all.at[owner, s],
-            send_sem=fan_send.at[kind, s],
-            recv_sem=fan_recv.at[kind, s],
-            device_id={"tp": peer},
-            device_id_type=MESH,
-        )
-
-    fan(1, t, e, across).start()
-    fan(0, t, e, mate).start()
-
-    def forward(i, carry):
-        s = lax.rem(e + n_ep - 1 - i, n_ep)
-        ep_copy(1, own_mixed.at[s], own_mixed.at[s], i, s).wait_recv()
-        fan(1, t, s, across).start()
-        fan(0, t, s, mate).start()
-        return carry
-
-    lax.fori_loop(0, n_ep - 1, forward, 0)
-
-    def relay(i, carry):
-        s = lax.rem(e + n_ep - i, n_ep)
-        fan(1, across, s, across).wait_recv()
-        fan(2, across, s, mate).start()
-        return carry
-
-    lax.fori_loop(0, n_ep, relay, 0)
+    from_line(1)
+    from_side(0)
+    from_across(0, 0)
+    from_line(2)
+    from_line(3)
     arrive(ep_copy, 0, ids_all, e, n_ep)
+    wanted = e.astype(F32)
+    hot = (ids_all[:, 0, 0:rows] == wanted).astype(F32) + (
+        ids_all[:, 1, 0:rows] == wanted
+    ).astype(F32)
+    rank = mm(hot.astype(BF16), later).astype(jnp.int32)
     down_k = lax.broadcasted_iota(jnp.int32, (cap, rows), 0)
-    wanted = e.astype(F32)
-
-    def take_group(i, carry):
-        s = lax.rem(e + n_ep - i, n_ep)
-        hot = (ids_all[s] == wanted).astype(F32)[0:2, 0:rows]
-        hot = hot[0:1] + hot[1:2]
-        rank = mm(jnp.broadcast_to(hot, (8, rows)).astype(BF16), later)[0:1].astype(jnp.int32)
-        pick = ((down_k == rank).astype(F32) * hot).astype(BF16)
-        fan(0, mate, s, mate).wait_recv()
-        fan(2, corner, s, mate).wait_recv()
-        normed2 = full_norm([mixed_all[c, s] for c in range(n_tp)], ffn_gain)
-        norm_s[...] = normed2
-        piece_s[s] = norm_s[pl.ds(pl.multiple_of(t * block, block), block), :]
-        moe_rows[s] = mm(pick, normed2.astype(BF16)).astype(BF16)
-        return carry
-
-    lax.fori_loop(0, n_ep, take_group, 0)
+    down_b = lax.broadcasted_iota(jnp.int32, (block, rows), 0)
+    along_b = lax.broadcasted_iota(jnp.int32, (block, rows), 1)
+    mine = (along_b == down_b + t * block).astype(F32)
+    for s in range(n_ep):
+        pick_s[s, :cap, :] = (down_k == rank[s : s + 1]).astype(F32) * hot[s : s + 1]
+        pick_s[s, cap:, :] = mine
+    from_side(1)
+    from_across(1, 0)
+    from_across(0, 1)
+    from_side(2)
+    from_side(3)
+    take_group(0, 0)
+    from_across(2, 0)
+    from_across(3, 0)
+    from_across(1, 1)
+    take_group(1, 0)
+    from_across(2, 1)
+    take_group(0, 1)
+    from_across(3, 1)
+    take_group(1, 1)
+    take_group(2, 0)
+    take_group(3, 0)
+    take_group(2, 1)
+    take_group(3, 1)
 
     for load in loads[6:9]:
         load.wait()
     piece = piece_s[...].reshape(n_ep * block, n_tp * width).astype(BF16)
     dense_hidden = (jax.nn.silu(mm(piece, dg[...])) * mm(piece, du[...])).astype(BF16)
-    dense_cols = min(512, dd.shape[1])
-
-    def dense_down(i, carry):
-        cols = pl.ds(pl.multiple_of(i * dense_cols, dense_cols), dense_cols)
+    half = dd.shape[1] // 2
+    places = [(k, side) for k in (3, 2, 1, 0) for side in (1, 0)][:-1]
+
+    def dense_copy(k, side, part):
+        cols = pl.ds(part * half, half)
+        return pltpu.make_async_remote_copy(
+            src_ref=dpart_send.at[2 * k + side, :, cols],
+            dst_ref=dpart_recv.at[e, :, cols],
+            send_sem=dense_send.at[part, 2 * k + side],
+            recv_sem=dense_recv.at[part, e],
+            device_id={"ep": here(k, side)},
+            device_id_type=MESH,
+        )
+
+    def dense_take(k, side, part):
+        cols = pl.ds(part * half, half)
+        s = here(k, side)
+        return pltpu.make_async_remote_copy(
+            src_ref=dpart_send.at[2 * k + side, :, cols],
+            dst_ref=dpart_recv.at[s, :, cols],
+            send_sem=dense_send.at[part, 2 * k + side],
+            recv_sem=dense_recv.at[part, s],
+            device_id={"ep": s},
+            device_id_type=MESH,
+        )
+
+    for part in range(2):
+        cols = slice(part * half, (part + 1) * half)
         value = mm(dense_hidden, dd[:, cols])
-        dpart_send[:, :, cols] = value.reshape(n_ep, block, dense_cols).astype(BF16)
-        return carry
-
-    lax.fori_loop(0, dd.shape[1] // dense_cols, dense_down, 0)
-    exchange(ep_copy, 2, lambda p: dpart_send.at[p], dpart_recv, e, n_ep)
-    dpart_recv[e] = dpart_send[e]
+        dpart_send[:, :, cols] = value.reshape(n_ep, block, half).astype(BF16)
+        for k, side in places:
+            dense_copy(k, side, part).start()
+    dpart_recv[e] = dpart_send[0]
 
     for load in loads[9:11]:
         load.wait()
@@ -549,14 +776,18 @@
         return carry
 
     lax.fori_loop(0, 2, to_mate_step, 0)
-    pair = pltpu.make_async_remote_copy(
-        src_ref=pair_send,
-        dst_ref=pair_recv,
-        send_sem=tp_send.at[3, 0],
-        recv_sem=tp_recv.at[3, 0],
-        device_id={"tp": across},
-        device_id_type=MESH,
-    )
+    band = n_ep * cap // 2
+
+    def pair(i):
+        some = pl.ds((1 - i) * band, band)
+        return pltpu.make_async_remote_copy(
+            src_ref=pair_send.at[some],
+            dst_ref=pair_recv.at[some],
+            send_sem=tp_send.at[3, i],
+            recv_sem=tp_recv.at[3, i],
+            device_id={"tp": across},
+            device_id_type=MESH,
+        )
 
     def own_step(i, carry):
         value = expert_down(lax.rem(t + 2 - 2 * i, n_tp))
@@ -566,59 +797,102 @@
         @pl.when(i == 0)
         def _():
             pair_send[...] = own_s[0].astype(BF16)
-            pair.start()
+            pair(0).start()
+            pair(1).start()
 
         return carry
 
     lax.fori_loop(0, 2, own_step, 0)
 
-    arrive(ep_copy, 2, dpart_recv, e, n_ep)
+    tp_left(0, x_all)
+    tp_left(1, heads_all)
+    sent(ep_copy, 0, lambda p: ids_all.at[e], ids_all, e, n_ep)
+    for k in (1, 2, 3):
+        along(k).wait_send()
+        aside(k - 1).wait_send()
+
+    @pl.when(at_end)
+    def _():
+        far().wait_send()
+
+    @pl.when(jnp.logical_not(at_end))
+    def _():
+        aside(3).wait_send()
+
+    for k in range(4):
+        for side in range(2):
+            over_y(k, side).wait_send()
+            to_core(k, side, t, 0).wait_send()
+            to_core(k, side, across, 1).wait_send()
+
+    def ret_copy(k, side):
+        return pltpu.make_async_remote_copy(
+            src_ref=ret_send.at[2 * k + side],
+            dst_ref=ret_recv.at[e],
+            send_sem=ep_send.at[1, 2 * k + side - 1],
+            recv_sem=give_recv.at[e],
+            device_id={"ep": here(k, side)},
+            device_id_type=MESH,
+        )
+
+    def ret_take(k, side):
+        s = here(k, side)
+        return pltpu.make_async_remote_copy(
+            src_ref=ret_send.at[2 * k + side],
+            dst_ref=ret_recv.at[s],
+            send_sem=ep_send.at[1, 2 * k + side - 1],
+            recv_sem=give_recv.at[s],
+            device_id={"ep": s},
+            device_id_type=MESH,
+        )
+
+    for i in range(2):
+        pair(i).wait_recv()
+        some = slice((1 - i) * band, (2 - i) * band)
+        summed = (own_s[1, some] + pair_recv[some].astype(F32)).astype(BF16)
+        ret_send[(1 - i) * n_ep // 2 : (2 - i) * n_ep // 2] = summed.reshape(
+            n_ep // 2, cap, width
+        )
+        for k, side in places:
+            if k // 2 == 1 - i:
+                ret_copy(k, side).start()
+    ret_recv[e] = ret_send[0]
+    for part in range(2):
+        for k, side in places[::-1]:
+            dense_take(k, side, part).wait_recv()
     dense_own = sum(dpart_recv[c].astype(F32) for c in range(n_ep))
     for c in range(n_tp):
         dfin_send[c] = dense_own[:, c * width : (c + 1) * width].astype(BF16)
     exchange(tp_copy, 4, lambda p: dfin_send.at[p], dfin_recv, t, n_tp)
     dfin_recv[t] = dfin_send[t]
 
-    pair.wait_recv()
-    summed = (own_s[1] + pair_recv[...].astype(F32)).astype(BF16)
-    ret_send[...] = summed.reshape(ret_send.shape)
-    exchange(ep_copy, 3, lambda p: ret_send.at[p], ret_recv, e, n_ep)
-    ret_recv[e] = ret_send[e]
     arrive(tp_copy, 4, dfin_recv, t, n_tp)
     dense_out = dfin_recv[...].astype(F32).reshape(rows, width)
     base = mixed.astype(F32) + jax.nn.sigmoid(dense_mix[...]) * dense_out
     high = take_matrix.astype(BF16)
     low = (take_matrix - high.astype(F32)).astype(BF16)
-    arrive(ep_copy, 3, ret_recv, e, n_ep)
+    sent(tp_copy, 4, lambda p: dfin_send.at[p], dfin_recv, t, n_tp)
+    for k, side in places:
+        for part in range(2):
+            dense_copy(k, side, part).wait_send()
+    pair(0).wait_send()
+    pair(1).wait_send()
+
+    def sent_mate(i, carry):
+        to_mate(i).wait_send()
+        return carry
+
+    lax.fori_loop(0, 2, sent_mate, 0)
+    for k, side in places[::-1]:
+        ret_take(k, side).wait_recv()
     returned = ret_recv[...].reshape(columns, width)
     over = (((0,), (0,)), ((), ()))
     moe_sum = lax.dot_general(
         high, returned, over, preferred_element_type=F32
     ) + lax.dot_general(low, returned, over, preferred_element_type=F32)
     out[...] = (base + moe_sum).astype(BF16)
-
-    sent(tp_copy, 0, lambda p: x_all.at[t], x_all, t, n_tp)
-    sent(tp_copy, 1, lambda p: heads_all.at[t], heads_all, t, n_tp)
-    sent(tp_copy, 4, lambda p: dfin_send.at[p], dfin_recv, t, n_tp)
-    sent(ep_copy, 0, lambda p: ids_all.at[e], ids_all, e, n_ep)
-    sent(ep_copy, 1, lambda p: own_mixed.at[e], own_mixed, e, n_ep)
-    sent(ep_copy, 2, lambda p: dpart_send.at[p], dpart_recv, e, n_ep)
-    sent(ep_copy, 3, lambda p: ret_send.at[p], ret_recv, e, n_ep)
-    pair.wait_send()
-
-    def sent_mate(i, carry):
-        to_mate(i).wait_send()
-        return carry
-
-    lax.fori_loop(0, 2, sent_mate, 0)
-
-    def sent_fan(s, carry):
-        fan(0, t, s, mate).wait_send()
-        fan(1, t, s, across).wait_send()
-        fan(2, across, s, mate).wait_send()
-        return carry
-
-    lax.fori_loop(0, n_ep, sent_fan, 0)
+    for k, side in places:
+        ret_copy(k, side).wait_send()
 
 
 def store_kernel(res, state, out, state_out, sem):
@@ -688,6 +962,15 @@
         return vmem(array.shape, array.dtype)
 
     scratch = [
+        vmem((1, model), F32),
+        vmem(w_beta.shape[::-1], BF16),
+        vmem(w_decay.shape[::-1], BF16),
+        vmem((1, decay_scale.shape[0]), F32),
+        vmem((1, head_gain.shape[0]), F32),
+        vmem((1, model), F32),
+        vmem(expert_ids.shape[::-1], expert_ids.dtype),
+        vmem(route_weight.shape[::-1], F32),
+        vmem((1, dense_mix.shape[0]), F32),
         like(w_query),
         like(w_key),
         like(w_value),
@@ -703,9 +986,9 @@
         *[vmem(head_shape, F32) for _ in range(7)],
         vmem((n_tp, rows, lh * dv), BF16),
         vmem((n_tp, n_ep, rows, width), BF16),
-        vmem((rows, model), F32),
         vmem((n_ep, block, model), F32),
         vmem((n_ep, cap, model), BF16),
+        vmem((n_ep, cap + block, rows), F32),
         vmem((n_ep, 8, 128), F32),
         vmem((n_ep, block, model), BF16),
         vmem((n_ep, block, model), BF16),
@@ -719,13 +1002,21 @@
         vmem((n_ep * cap, width), BF16),
         vmem((n_ep, cap, width), BF16),
         vmem((n_ep, cap, width), BF16),
+        pltpu.SemaphoreType.DMA((10,)),
         pltpu.SemaphoreType.DMA((12,)),
         pltpu.SemaphoreType.DMA((5, n_tp - 1)),
         pltpu.SemaphoreType.DMA((5, n_tp - 1)),
         pltpu.SemaphoreType.DMA((4, n_ep - 1)),
         pltpu.SemaphoreType.DMA((4, n_ep - 1)),
-        pltpu.SemaphoreType.DMA((3, n_ep)),
-        pltpu.SemaphoreType.DMA((3, n_ep)),
+        pltpu.SemaphoreType.DMA((4,)),
+        pltpu.SemaphoreType.DMA((4,)),
+        pltpu.SemaphoreType.DMA((4, 2)),
+        pltpu.SemaphoreType.DMA((2, 4, 2)),
+        pltpu.SemaphoreType.DMA((n_tp, n_ep)),
+        pltpu.SemaphoreType.DMA((2, n_ep)),
+        pltpu.SemaphoreType.DMA((2, n_ep)),
+        pltpu.SemaphoreType.DMA((n_ep,)),
+        pltpu.SemaphoreType.REGULAR((3,)),
     ]
     return store_outputs(
         *pl.pallas_call(
@@ -734,7 +1025,7 @@
                 pltpu.VMEM(hidden_in.shape, BF16),
                 pltpu.VMEM(state_in.shape, F32),
             ),
-            in_specs=[whole] * 10 + [away] * 12,
+            in_specs=[away] * 22,
             out_specs=(whole, whole),
             scratch_shapes=scratch,
             compiler_params=pltpu.CompilerParams(
@@ -781,7 +1072,7 @@
         and (rows // n_tp) % 8 == 0
         and width % 128 == 0
         and args[15].shape[2] % 256 == 0
-        and n_ep <= 128
+        and n_ep == 8
     )
     if fits:
         return fused_device(n_ep, n_tp, *args)

time: 49.5 us -> 43.2 us (0.87)
  Pallas kernels: 48.7 us -> 42.4 us
    pallas_call x1, Pallas kernels: 46.7 us -> 40.3 us  [fused_device(): pl.pallas_call(functools.partial(layer_kernel, (n_ep, n_tp, rows, lh, dk,...]
where the time goes in v2:
time: 43.2 us; the launch traced here: 43 us
  Pallas kernels  42.4 us (98%)
  between operations  0.65 us (2%)
    pallas_call x1, Pallas kernels, fused_device(): pl.pallas_call(functools.partial(layer_kernel, (n_ep, n_tp, rows, lh, dk,...  40.3 us
    pallas_call x1, Pallas kernels, store_outputs(): pl.pallas_call(store_kernel, out_shape=(jax.ShapeDtypeStruct(res.shape, r...  2.04 us

profile of v2, /device:TPU:0, one launch (start us, length us, event | category | flops | bytes accessed | tf_op | source)
XLA Modules:
  0.0 43.0 jit_solution(16443511167273437155)
XLA Ops:
  0.6 40.3 %shard_map.221 = (bf16[32,512]{1,0:T(8,128)(2,1)S(1)}, f32[32,2,128,128]{3,2,1,0:T(8,128)S(1)}) custom-call(bf16[32,512]{1,0:T(8,128)(2,1)} %hidden_hbm.1, f32[1,2048]{1,0:T(1,128)} %bitcast.11, bf16[8,2048]{1,0:T(8,128)(2,1)} %bitcast.9, bf16[8,2048]{1,0:T(8,128)(2,1)} %bitcast.10, f32[1,8]{1,0:T(1,128)} %bitcast.16, f32[1,128]{1,0:T(1,128)} %bitcast.17, ...), custom_call_target="tpu_custom_call" | custom-call | tf_op jit(solution)/shard_map/pallas_call | solution.py:1022
  41.0 2.0 %shard_map.222 = (bf16[32,512]{1,0:T(8,128)(2,1)}, f32[32,2,128,128]{3,2,1,0:T(8,128)}) custom-call(bf16[32,512]{1,0:T(8,128)(2,1)S(1)} %get-tuple-element.4.res, f32[32,2,128,128]{3,2,1,0:T(8,128)S(1)} %get-tuple-element.5.state), custom_call_target="tpu_custom_call" | custom-call | tf_op jit(solution)/shard_map/pallas_call | solution.py:912
